TPU v7x, 32 devices: a whole 2x2x4 slice. The times are simulated.
32 devices in a mesh: grp: 2 (over y), sp: 4 (over z), fs: 2 (over x), tp: 2 (over core).
Axes of the slice: x: 2, y: 2, z: 4, core: 2. Of those that a mesh axis runs over, the one named last changes fastest.
Arguments:
- tokens: bfloat16 [2, 6144, 2048], P('fs', ('grp', 'sp'), 'tp'), parts along dimension 1, may hold values from -12 to 12
- norm_gain: float32 [2048], replicated, may hold values from 0.1 to 1.9
- query_weight: bfloat16 [2048, 16, 64], P(None, 'tp'), may hold values from -3 to 3
- key_weight: bfloat16 [2048, 4, 64], P(None, 'tp'), may hold values from -3 to 3
- value_weight: bfloat16 [2048, 4, 64], P(None, 'tp'), may hold values from -0.125 to 0.125
- sink_logit: float32 [16], P('tp'), may hold values from 1 to 6
- pool_weight: bfloat16 [2048, 4, 256], P(None, None, 'tp'), may hold values from -0.125 to 0.125
- attn_out_weight: bfloat16 [16, 64, 2048], P('tp'), may hold values from -0.5 to 0.5
- pool_out_weight: bfloat16 [4, 256, 2048], P(None, 'tp'), may hold values from -0.1875 to 0.1875
Outputs:
- mixed: bfloat16 [2, 6144, 2048], P('fs', ('grp', 'sp', 'tp')), parts along dimension 1
There are 2 independent parts, one for each index of `grp`. A program takes and returns all parts, laid end to end along the dimension named above; an argument that names none is the same for every part. Nothing has to cross between parts.
All inputs are finite; a program needn't handle non-finite values.
Results may differ from a plain program's by a relative error of at most 0.0095.
The roundings to bfloat16 on the way count: a program that leaves them out, or rounds other values in their place, can miss the bound.
Values may be sent and summed in bfloat16 or wider, within the bound.
No kernel may reach another device: no remote copies, remote signals or barrier semaphores. Data moves between devices by JAX's collectives and lax.ppermute only.
A program may use at most 128 MiB of HBM per device.

v0:
```python
import jax
import jax.numpy as jnp
from jax import lax
from jax.sharding import PartitionSpec as P

WINDOW = 128


def from_behind(value, axis, steps):
    count = lax.axis_size(axis)
    first, last = (max(0, -steps), min(count, count - steps))
    return lax.ppermute(value, axis, [(source, source + steps) for source in range(first, last)])


def rms_norm(rows, gain):
    values = rows.astype(jnp.float32)
    scale = lax.rsqrt(jnp.mean(values * values, axis=-1, keepdims=True) + 1e-06)
    return (values * scale * gain).astype(jnp.bfloat16)


def attend(query, key, value, key_tail, value_tail, sinks, offset):
    rows = query.shape[0]
    local_kv = key_tail.shape[1]
    head_dim = key_tail.shape[2]
    group = query.shape[1] // (local_kv * head_dim)
    blocks = rows // WINDOW
    qb = query.reshape(blocks, WINDOW, local_kv, group, head_dim)

    def banded(tensor, tail):
        tb = tensor.reshape(blocks, WINDOW, local_kv, head_dim)
        whole = jnp.concatenate([tail, tensor.reshape(rows, local_kv, head_dim)], axis=0)
        before = whole[:rows].reshape(blocks, WINDOW, local_kv, head_dim)
        return jnp.concatenate([before, tb], axis=1)

    kw = banded(key, key_tail)
    vw = banded(value, value_tail)
    qi = jnp.arange(WINDOW, dtype=jnp.int32)[:, None]
    kj = jnp.arange(2 * WINDOW, dtype=jnp.int32)[None, :]
    dist = WINDOW + qi - kj
    inside = (dist >= 0) & (dist < WINDOW)
    key_pos = (
        offset + jnp.arange(blocks, dtype=jnp.int32)[:, None, None] * WINDOW - WINDOW + kj[None]
    )
    mask = inside[None] & (key_pos >= 0)
    scores = jnp.einsum(
        "nqhgd,nkhd->nhgqk", qb, kw, preferred_element_type=jnp.float32
    ) * head_dim ** (-0.5)
    scores = jnp.where(mask[:, None, None], scores, -jnp.inf)
    sink = sinks.reshape(1, local_kv, group, 1, 1)
    top = jnp.maximum(jnp.max(scores, axis=-1, keepdims=True), sink)
    expo = jnp.exp(scores - top)
    total = jnp.sum(expo, axis=-1, keepdims=True) + jnp.exp(sink - top)
    weight = (expo / total).astype(jnp.bfloat16)
    out = jnp.einsum("nhgqk,nkhd->nqhgd", weight, vw, preferred_element_type=jnp.float32)
    return out.reshape(rows, -1).astype(jnp.bfloat16)


def shards(
    tokens,
    norm_gain,
    query_weight,
    key_weight,
    value_weight,
    sink_logit,
    pool_weight,
    attn_out_weight,
    pool_out_weight,
):
    whole = lax.all_gather(tokens, "tp", axis=2, tiled=True)[0]
    rows = whole.shape[0]
    width = whole.shape[1]
    local_kv = key_weight.shape[1]
    head_dim = key_weight.shape[2]
    channels = pool_weight.shape[2]
    normed = rms_norm(whole, norm_gain)
    query = jnp.dot(
        normed, query_weight.reshape(width, -1), preferred_element_type=jnp.float32
    ).astype(jnp.bfloat16)
    key = jnp.dot(normed, key_weight.reshape(width, -1), preferred_element_type=jnp.float32).astype(
        jnp.bfloat16
    )
    value = jnp.dot(
        normed, value_weight.reshape(width, -1), preferred_element_type=jnp.float32
    ).astype(jnp.bfloat16)
    pooled_in = jnp.dot(
        normed, pool_weight.reshape(width, -1), preferred_element_type=jnp.float32
    ).astype(jnp.bfloat16)
    pool_rows = pooled_in.reshape(rows, 4, channels)
    key_rows = key.reshape(rows, local_kv, head_dim)
    value_rows = value.reshape(rows, local_kv, head_dim)
    key_tail, value_tail, pool_tail = from_behind(
        (key_rows[rows - WINDOW :], value_rows[rows - WINDOW :], pool_rows[rows - WINDOW :]),
        "sp",
        1,
    )
    offset = lax.axis_index("sp") * rows
    attended = attend(query, key, value, key_tail, value_tail, sink_logit, offset)
    prefix_total = jnp.sum(pool_rows[:, 3].astype(jnp.float32), axis=0)
    totals = lax.all_gather(prefix_total[None], "sp", axis=0, tiled=True)
    below = jnp.arange(totals.shape[0], dtype=jnp.int32) < lax.axis_index("sp")
    carried = jnp.sum(jnp.where(below[:, None], totals, 0.0), axis=0)
    reaches = jnp.array([2.0, 4.0, 16.0, 1000000000.0], jnp.float32)
    ext = jnp.concatenate([pool_tail, pool_rows], axis=0)
    position = jnp.arange(rows, dtype=jnp.int32)[:, None]
    source = jnp.arange(rows + WINDOW, dtype=jnp.int32)[None, :]
    gap = (position + WINDOW - source).astype(jnp.float32)
    group_ids = jnp.arange(4, dtype=jnp.int32)[:, None, None]
    band = (
        (gap[None] >= 0.0)
        & (gap[None] < reaches[:, None, None])
        & ((group_ids < 3) | (source[None] >= WINDOW))
    )
    sums = jnp.einsum(
        "gij,jgc->igc", band.astype(jnp.bfloat16), ext, preferred_element_type=jnp.float32
    )
    carry_rows = jnp.concatenate([jnp.zeros((3, channels), jnp.float32), carried[None]], axis=0)
    sums = sums + carry_rows[None]
    count = (offset + jnp.arange(1, rows + 1, dtype=jnp.int32)).astype(jnp.float32)
    denom = jnp.minimum(count[:, None], reaches[None, :])[:, :, None]
    pooled = (
        (sums / denom - pool_rows.astype(jnp.float32))
        .astype(jnp.bfloat16)
        .reshape(rows, 4 * channels)
    )
    attn_rows = attn_out_weight.reshape(-1, width)
    pool_weight_rows = pool_out_weight.reshape(-1, width)
    part_sum = jnp.dot(attended, attn_rows, preferred_element_type=jnp.float32)
    result = lax.psum_scatter(
        (part_sum + jnp.dot(pooled, pool_weight_rows, preferred_element_type=jnp.float32)).astype(
            jnp.bfloat16
        ),
        "tp",
        scatter_dimension=0,
        tiled=True,
    )
    return result[None]


def solution(mesh):
    in_specs = (
        P("fs", ("grp", "sp"), "tp"),
        P(),
        P(None, "tp", None),
        P(None, "tp", None),
        P(None, "tp", None),
        P("tp"),
        P(None, None, "tp"),
        P("tp", None, None),
        P(None, "tp", None),
    )
    out_specs = P("fs", ("grp", "sp", "tp"), None)
    return jax.shard_map(shards, mesh=mesh, in_specs=in_specs, out_specs=out_specs, check_vma=False)
```

profile of v0, /device:TPU:0, one launch (start us, length us, event | category | flops | bytes accessed | tf_op | source)
XLA Modules:
  0.0 103.8 jit_solution(3450044622372322319)
XLA Ops:
  7.3 0.7 max.18
  8.8 0.7 broadcast_minimum_fusion
  9.9 1.5 %broadcast_compare_fusion = pred[768,896]{1,0:T(8,128)(4,1)} fusion(s32[768]{0:T(1024)S(1)} %iota_add_fusion), kind=kLoop, calls=%fused_computation.34 | loop fusion | flops 2064384 | bytes 691200 | tf_op jit(solution)/shard_map/ge | solution.py:109
  11.4 1.8 %subtract_convert_fusion = f32[768,896]{1,0:T(8,128)} fusion(s32[768]{0:T(1024)S(1)} %iota_add_fusion), kind=kLoop, calls=%fused_computation.22 | loop fusion | flops 1376256 | bytes 2755584 | tf_op jit(solution)/shard_map/convert_element_type | solution.py:106
  13.1 10.6 %all-gather.4.cloned.1.call-done = bf16[1,768,2048]{2,1,0:T(8,128)(2,1)} async-done(((bf16[1,768,1024]{2,1,0:T(8,128)(2,1)}), bf16[1,768,2048]{2,1,0:T(8,128)(2,1)}) %all-gather.4.cloned.1.call-update) | async-done | bytes 3145744 | tf_op jit(solution)/shard_map/all_gather | solution.py:69
  23.8 2.7 %fusion.4 = f32[768]{0:T(1024)S(1)} fusion(bf16[1,768,2048]{2,1,0:T(8,128)(2,1)} %all-gather.4.cloned.1.call-done), kind=kLoop, calls=%fused_computation.6 | loop fusion | flops 4717824 | bytes 3148800 | tf_op jit(solution)/shard_map/reduce_sum | solution.py:17
  26.6 2.3 %convolution_convert_fusion.2 = bf16[768,128]{0,1:T(8,128)(2,1)S(1)} fusion(bf16[2048,128]{0,1:T(8,128)(2,1)} %bitcast.105, bf16[1,768,2048]{2,1,0:T(8,128)(2,1)S(1)} %copy-done.1, f32[2048]{0:T(1024)S(1)} %copy-done.10, f32[768]{0:T(1024)S(1)} %add_rsqrt_fusion), kind=kOutput, calls=%fused_computation.37 | convolution fusion | flops 409042944 | bytes 3877888 | tf_op jit(solution)/shard_map/dot_general | solution.py:82
  29.2 3.4 %convolution_convert_fusion.1 = bf16[768,128]{0,1:T(8,128)(2,1)S(1)} fusion(bf16[2048,128]{0,1:T(8,128)(2,1)} %bitcast.106, bf16[1,768,2048]{2,1,0:T(8,128)(2,1)} %all-gather.4.cloned.1.call-done, f32[2048]{0:T(1024)S(1)} %copy-done.10, f32[768]{0:T(1024)S(1)} %add_rsqrt_fusion), kind=kOutput, calls=%fused_computation.36 | convolution fusion | flops 409042944 | bytes 3877888 | tf_op jit(solution)/shard_map/dot_general | solution.py:79
  32.6 4.3 %collective-permute-start.1 = (bf16[128,2,64]{0,2,1:T(8,128)(2,1)S(1)}, bf16[128,2,64]{0,2,1:T(8,128)(2,1)}, u32[]{:S(2)}, u32[]{:S(2)}) collective-permute-start(bf16[128,2,64]{0,2,1:T(8,128)(2,1)S(1)} %bitcast.99), channel_id=1, source_target_pairs={{0,4},{4,8},{8,12},{1,5},{5,9},{9,13},{2,6},{6,10},{10,14},{3,7},{... | collective-permute-start | bytes 98312 | tf_op jit(solution)/shard_map/ppermute | solution.py:12
  36.9 3.4 %collective-permute-start = (bf16[128,2,64]{0,2,1:T(8,128)(2,1)S(1)}, bf16[128,2,64]{0,2,1:T(8,128)(2,1)}, u32[]{:S(2)}, u32[]{:S(2)}) collective-permute-start(bf16[128,2,64]{0,2,1:T(8,128)(2,1)S(1)} %bitcast.98), channel_id=1, source_target_pairs={{0,4},{4,8},{8,12},{1,5},{5,9},{9,13},{2,6},{6,10},{10,14},{3,7},{... | collective-permute-start | bytes 98312 | tf_op jit(solution)/shard_map/ppermute | solution.py:12
  40.3 2.0 %fusion.25 = bf16[768,512]{0,1:T(8,128)(2,1)S(1)} fusion(bf16[256,8,4,128]{3,2,1,0:T(4,128)(2,1)S(1)} %bitcast.103, bf16[1,768,2048]{2,1,0:T(8,128)(2,1)S(1)} %copy-done.2, f32[2048]{0:T(1024)S(1)} %copy-done.10, f32[768]{0:T(1024)S(1)} %add_rsqrt_fusion), kind=kOutput, calls=%fused_computation.31 | convolution fusion | flops 1617297408 | bytes 6040576 | tf_op jit(solution)/shard_map/dot_general | solution.py:85
  42.5 8.5 %all-gather.1 = f32[4,1,128]{2,1,0:T(1,128)S(1)} all-gather(f32[1,1,128]{2,1,0:T(1,128)S(1)} %bitcast.101), channel_id=2, replica_groups=mesh['grp'=2,'sp'=4,'fs'=2,'tp'=2] {'sp'}, dimensions={0}, use_global_device_ids=true | all-gather | bytes 2560 | tf_op jit(solution)/shard_map/all_gather | solution.py:99
  50.9 3.7 %collective-permute-start.2 = (bf16[128,4,128]{0,2,1:T(8,128)(2,1)S(1)}, bf16[128,4,128]{0,2,1:T(8,128)(2,1)}, u32[]{:S(2)}, u32[]{:S(2)}) collective-permute-start(bf16[128,4,128]{0,2,1:T(8,128)(2,1)S(1)} %bitcast.97), channel_id=1, source_target_pairs={{0,4},{4,8},{8,12},{1,5},{5,9},{9,13},{2,6},{6,10},{10,14},{3,7},{... | collective-permute-start | bytes 393224 | tf_op jit(solution)/shard_map/ppermute | solution.py:12
  54.6 2.7 %convolution_convert_fusion = bf16[768,512]{1,0:T(8,128)(2,1)} fusion(bf16[2048,512]{0,1:T(8,128)(2,1)S(1)} %bitcast.104, bf16[1,768,2048]{2,1,0:T(8,128)(2,1)S(1)} %copy-done.2, f32[2048]{0:T(1024)S(1)} %copy-done.10, f32[768]{0:T(1024)S(1)} %add_rsqrt_fusion), kind=kOutput, calls=%fused_computation.32 | convolution fusion | flops 1617297408 | bytes 6040576 | tf_op jit(solution)/shard_map/dot_general | solution.py:76
  58.3 3.6 %reshape.334 = bf16[6,128,2,4,64]{4,3,2,1,0:T(4,128)(2,1)} reshape(bf16[768,512]{1,0:T(8,128)(2,1)} %convolution_convert_fusion) | data formatting | bytes 1572864 | tf_op jit(solution)/shard_map/reshape | solution.py:27
  61.9 1.3 %concatenate.23 = f32[4,128]{1,0:T(4,128)} pad(f32[1,128]{1,0:T(1,128)} %bitcast.102, f32[]{:T(128)} %constant.14.clone.1), padding=3_0x0_0 | pad | bytes 2564 | tf_op jit(solution)/shard_map/concatenate | solution.py:116
  63.2 0.8 copy_bitcast_fusion
  64.0 2.7 %fusion.13 = (f32[6,2,4,128]{3,2,1,0:T(4,128)S(1)}, f32[6,2,256,128,4]{3,2,4,1,0:T(8,128)S(1)}) fusion(pred[6,128,256]{1,2,0:T(8,128)(4,1)S(1)} %broadcast_and_fusion, bf16[6,128,2,4,64]{4,3,2,1,0:T(4,128)(2,1)} %reshape.334, bf16[6,128,2,64]{1,3,2,0:T(8,128)(2,1)S(1)} %copy.28, bf16[6,128,2,64]{1,3,2,0:T(8,128)(2,1)S(1)} %copy_bitcast_fusion), kind=kOutput, calls=%fused_computation.19 | convolution fusion | flops 206825472 | bytes 7692288 | tf_op jit(solution)/shard_map/nqhgd,nkhd->nhgqk/dot_general | solution.py:45
  66.8 1.7 %fusion.8 = f32[6,2,4,128]{3,2,1,0:T(4,128)S(1)} fusion(f32[6,2,256,128,4]{3,2,4,1,0:T(8,128)S(1)} %get-tuple-element.6, f32[6,2,4,128]{3,2,1,0:T(4,128)S(1)} %broadcast_maximum_fusion, pred[6,128,256]{1,2,0:T(8,128)(4,1)S(1)} %broadcast_and_fusion), kind=kLoop, calls=%fused_computation.14 | loop fusion | flops 6285312 | bytes 6537216 | tf_op jit(solution)/shard_map/reduce_sum | solution.py:52
  68.5 0.8 copy_bitcast_fusion.1
  69.3 1.7 %fusion.31 = bf16[6,128,2,4,64]{1,4,3,2,0:T(8,128)(2,1)S(1)} fusion(f32[6,2,256,128,4]{3,2,4,1,0:T(8,128)S(1)} %get-tuple-element.6, f32[6,2,4,128]{3,2,1,0:T(4,128)S(1)} %exponential_add_fusion, f32[6,2,4,128]{3,2,1,0:T(4,128)S(1)} %broadcast_maximum_fusion, pred[6,128,256]{1,2,0:T(8,128)(4,1)S(1)} %broadcast_and_fusion, ...), kind=kOutput, calls=%fused_computation.35 | convolution fusion | flops 210370560 | bytes 7716864 | tf_op jit(solution)/shard_map/nhgqk,nkhd->nqhgd/dot_general | solution.py:54
  71.7 4.5 %fusion.38 = f32[768,2048]{1,0:T(8,128)} fusion(bf16[512,2048]{1,0:T(8,128)(2,1)S(1)} %bitcast.91, bf16[64,8,6,128]{3,2,1,0:T(8,128)(2,1)S(1)} %bitcast.92), kind=kOutput, calls=%fused_computation.41 | convolution fusion | flops 1610612736 | bytes 9175040 | tf_op jit(solution)/shard_map/dot_general | solution.py:127
  76.2 11.3 %fusion.7 = bf16[768,2048]{1,0:T(8,128)(2,1)} fusion(f32[768,2048]{1,0:T(8,128)} %fusion.38, bf16[4,128,2048]{2,1,0:T(8,128)(2,1)} %param.18, bf16[768,4,128]{0,2,1:T(8,128)(2,1)} %bitcast.96, f32[768,896]{1,0:T(8,128)} %subtract_convert_fusion, f32[4]{0:T(128)S(1)} %copy-done.7, pred[4,896]{1,0:T(4,128)(4,1)S(1)} %copy-done.5, ...), kind=kOutput, calls=%fused_computation.10 | convolution fusion | flops 2330460160 | bytes 15910416 | tf_op jit(solution)/shard_map/dot_general | solution.py:129
  87.5 9.5 %reduce-scatter.2.cloned.1.call-done = bf16[384,2048]{1,0:T(8,128)(2,1)} async-done(((bf16[768,2048]{1,0:T(8,128)(2,1)}), bf16[384,2048]{1,0:T(8,128)(2,1)}) %reduce-scatter.2.cloned.1.call-update) | async-done | bytes 1572880 | tf_op jit(solution)/shard_map/reduce_scatter | solution.py:128
  (53 shorter events, 4.1 us)
Async XLA Ops:
  6.5 65.1 %copy-start = (bf16[8,64,2048]{2,1,0:T(8,128)(2,1)S(1)}, bf16[8,64,2048]{2,1,0:T(8,128)(2,1)}, u32[]{:S(2)}) copy-start(bf16[8,64,2048]{2,1,0:T(8,128)(2,1)} %param.17) | copy-start | bytes 6291460
  6.5 17.2 %all-gather.4.cloned.1.call-start = ((), (), s32[]{:S(2)}) async-start(), calls=%async_computation.1 | async-start | bytes 4718592 | tf_op jit(solution)/shard_map/all_gather | solution.py:69
  7.3 89.7 %reduce-scatter.2.cloned.1.call-start = ((), (), s32[]{:S(2)}) async-start(), calls=%async_computation.2 | async-start | bytes 4718592 | tf_op jit(solution)/shard_map/reduce_scatter | solution.py:128
  9.9 16.6 %copy-start.10 = (f32[2048]{0:T(1024)S(1)}, f32[2048]{0:T(1024)}, u32[]{:S(2)}) copy-start(f32[2048]{0:T(1024)} %param.11) | copy-start | bytes 24580
  23.8 2.8 %copy-start.1 = (bf16[1,768,2048]{2,1,0:T(8,128)(2,1)S(1)}, bf16[1,768,2048]{2,1,0:T(8,128)(2,1)}, u32[]{:S(2)}) copy-start(bf16[1,768,2048]{2,1,0:T(8,128)(2,1)} %all-gather.4.cloned.1.call-done) | copy-start | bytes 9437188
  29.2 11.1 %copy-start.2 = (bf16[1,768,2048]{2,1,0:T(8,128)(2,1)S(1)}, bf16[1,768,2048]{2,1,0:T(8,128)(2,1)}, u32[]{:S(2)}) copy-start(bf16[1,768,2048]{2,1,0:T(8,128)(2,1)} %all-gather.4.cloned.1.call-done) | copy-start | bytes 9437188
  29.2 11.1 %copy-start.8 = (bf16[2048,4,128]{2,1,0:T(4,128)(2,1)S(1)}, bf16[2048,4,128]{2,1,0:T(4,128)(2,1)}, u32[]{:S(2)}) copy-start(bf16[2048,4,128]{2,1,0:T(4,128)(2,1)} %param.16) | copy-start | bytes 6291460
  32.6 30.6 %collective-permute-start.1 = (bf16[128,2,64]{0,2,1:T(8,128)(2,1)S(1)}, bf16[128,2,64]{0,2,1:T(8,128)(2,1)}, u32[]{:S(2)}, u32[]{:S(2)}) collective-permute-start(bf16[128,2,64]{0,2,1:T(8,128)(2,1)S(1)} %bitcast.99), channel_id=1, source_target_pairs={{0,4},{4,8},{8,12},{1,5},{5,9},{9,13},{2,6},{6,10},{10,14},{3,7},{... | collective-permute-start | bytes 98312 | tf_op jit(solution)/shard_map/ppermute | solution.py:12
  36.9 31.7 %collective-permute-start = (bf16[128,2,64]{0,2,1:T(8,128)(2,1)S(1)}, bf16[128,2,64]{0,2,1:T(8,128)(2,1)}, u32[]{:S(2)}, u32[]{:S(2)}) collective-permute-start(bf16[128,2,64]{0,2,1:T(8,128)(2,1)S(1)} %bitcast.98), channel_id=1, source_target_pairs={{0,4},{4,8},{8,12},{1,5},{5,9},{9,13},{2,6},{6,10},{10,14},{3,7},{... | collective-permute-start | bytes 98312 | tf_op jit(solution)/shard_map/ppermute | solution.py:12
  40.3 14.3 %copy-start.9 = (bf16[2048,8,64]{0,2,1:T(8,128)(2,1)S(1)}, bf16[2048,8,64]{0,2,1:T(8,128)(2,1)}, u32[]{:S(2)}) copy-start(bf16[2048,8,64]{0,2,1:T(8,128)(2,1)} %param.12) | copy-start | bytes 6291460
  42.3 15.0 %copy-start.4 = (bf16[768,512]{0,1:T(8,128)(2,1)}, bf16[768,512]{0,1:T(8,128)(2,1)S(1)}, u32[]{:S(2)}) copy-start(bf16[768,512]{0,1:T(8,128)(2,1)S(1)} %fusion.25) | copy-start | bytes 2359300
  50.9 25.2 %collective-permute-start.2 = (bf16[128,4,128]{0,2,1:T(8,128)(2,1)S(1)}, bf16[128,4,128]{0,2,1:T(8,128)(2,1)}, u32[]{:S(2)}, u32[]{:S(2)}) collective-permute-start(bf16[128,4,128]{0,2,1:T(8,128)(2,1)S(1)} %bitcast.97), channel_id=1, source_target_pairs={{0,4},{4,8},{8,12},{1,5},{5,9},{9,13},{2,6},{6,10},{10,14},{3,7},{... | collective-permute-start | bytes 393224 | tf_op jit(solution)/shard_map/ppermute | solution.py:12
  71.6 4.5 %copy-start.3 = (pred[768,896]{1,0:T(8,128)(4,1)S(1)}, pred[768,896]{1,0:T(8,128)(4,1)}, u32[]{:S(2)}) copy-start(pred[768,896]{1,0:T(8,128)(4,1)} %broadcast_compare_fusion) | copy-start | bytes 2064388
  71.7 4.5 %copy-start.5 = (pred[4,896]{1,0:T(4,128)(4,1)S(1)}, pred[4,896]{1,0:T(4,128)(4,1)}, u32[]{:S(2)}) copy-start(pred[4,896]{1,0:T(4,128)(4,1)} %broadcast_or_fusion) | copy-start | bytes 10756
  71.7 4.5 %copy-start.6 = (f32[4,128]{1,0:T(4,128)S(1)}, f32[4,128]{1,0:T(4,128)}, u32[]{:S(2)}) copy-start(f32[4,128]{1,0:T(4,128)} %concatenate.23) | copy-start | bytes 6148
  71.7 4.5 %copy-start.7 = (f32[4]{0:T(128)S(1)}, f32[4]{0:T(128)}, u32[]{:S(2)}) copy-start(f32[4]{0:T(128)} %constant.13.clone) | copy-start | bytes 52
Sparse Core Ops, SparseCore 0:
  8.9 14.8 all-gather.3
  87.7 9.2 reduce-scatter.1
where the time goes:
time: 104 us
  matrix products  30.6 us (29%)
  waiting for transfers between devices  20.8 us (20%)
  between operations  13.7 us (13%)
  other arithmetic  12 us (12%)
  starting transfers between devices  11.4 us (11%)
  blocking collectives  8.46 us (8%)
  local copies, waits for them, and re-layouts  6.9 us (7%)
    ppermute x3, starting transfers between devices, from_behind(): lax.ppermute(value, axis, [(source, source + steps) for source in range(f...  11.3 us
    dot_general x1, matrix products, shards(): jnp.dot(pooled, pool_weight_rows, preferred_element_type=jnp.float32)  11.3 us
    all_gather x1, waiting for transfers between devices, shards(): whole = lax.all_gather(tokens, 'tp', axis=2, tiled=True)[0]  10.6 us
    reduce_scatter x1, waiting for transfers between devices, shards(): lax.psum_scatter((part_sum + jnp.dot(pooled, pool_weight_rows, preferred_...  9.46 us
    all_gather x1, blocking collectives, shards(): totals = lax.all_gather(prefix_total[None], 'sp', axis=0, tiled=True)  8.46 us
    dot_general x1, matrix products, shards(): part_sum = jnp.dot(attended, attn_rows, preferred_element_type=jnp.float32)  4.48 us
    reshape x1, local copies, waits for them, and re-layouts, attend(): qb = query.reshape(blocks, WINDOW, local_kv, group, head_dim)  3.63 us
    dot_general x1, matrix products, shards(): jnp.dot(normed, key_weight.reshape(width, -1), preferred_element_type=jnp...  3.38 us
  transfers between devices with their start and end apart: 5, of which 2 were waited for; matrix products, arithmetic and copies ran while one was open for 28% of the time, Pallas kernels for 0%

commit v1 on v0

--- a/solution.py
+++ b/solution.py
@@ -66,7 +66,7 @@
     attn_out_weight,
     pool_out_weight,
 ):
-    whole = lax.all_gather(tokens, "tp", axis=2, tiled=True)[0]
+    whole = jnp.concatenate(lax.all_gather(tokens, "tp"), axis=2)[0]
     rows = whole.shape[0]
     width = whole.shape[1]
     local_kv = key_weight.shape[1]

time: 104 us -> 111 us (1.067)
  local copies, waits for them, and re-layouts: 6.9 us -> 13.8 us
  other arithmetic: 12 us -> 13.2 us
  waiting for transfers between devices: 20.8 us -> 19.6 us
    all_gather x0 -> x1, local copies, waits for them, and re-layouts: none -> 4.63 us  [shards(): whole = jnp.concatenate(lax.all_gather(tokens, 'tp'), axis=2)[0]]
    dot_general x1, matrix products: 2.32 us -> 0.59 us  [shards(): jnp.dot(normed, value_weight.reshape(width, -1), preferred_element_type=j...]
    dot_general x1, matrix products: 2.01 us -> 3.68 us  [shards(): jnp.dot(normed, pool_weight.reshape(width, -1), preferred_element_type=jn...]
    unnamed x22 -> x26, local copies, waits for them, and re-layouts: 0.14 us -> 1.79 us
    all_gather x1, waiting for transfers between devices: 10.6 us -> 9.43 us  [shards(): whole = jnp.concatenate(lax.all_gather(tokens, 'tp'), axis=2)[0]]
  transfers between devices with their start and end apart: 5 -> 5, of which waited for: 2 -> 2; matrix products, arithmetic and copies ran while one was open for 28% -> 31% of each run, Pallas kernels for 0% -> 0%
where the time goes in v1:
time: 111 us; the launch traced here: 110 us
  matrix products  29.7 us (27%)
  waiting for transfers between devices  19.6 us (18%)
  local copies, waits for them, and re-layouts  13.8 us (12%)
  between operations  13.7 us (12%)
  other arithmetic  13.2 us (12%)
  starting transfers between devices  11.7 us (11%)
  blocking collectives  8.46 us (8%)
    ppermute x3, starting transfers between devices, from_behind(): lax.ppermute(value, axis, [(source, source + steps) for source in range(f...  11.6 us
    dot_general x1, matrix products, shards(): jnp.dot(pooled, pool_weight_rows, preferred_element_type=jnp.float32)  11.3 us
    reduce_scatter x1, waiting for transfers between devices, shards(): lax.psum_scatter((part_sum + jnp.dot(pooled, pool_weight_rows, preferred_...  9.46 us
    all_gather x1, waiting for transfers between devices, shards(): whole = jnp.concatenate(lax.all_gather(tokens, 'tp'), axis=2)[0]  9.43 us
    all_gather x1, blocking collectives, shards(): totals = lax.all_gather(prefix_total[None], 'sp', axis=0, tiled=True)  8.46 us
    all_gather x1, local copies, waits for them, and re-layouts, shards(): whole = jnp.concatenate(lax.all_gather(tokens, 'tp'), axis=2)[0]  4.63 us
    dot_general x1, matrix products, shards(): part_sum = jnp.dot(attended, attn_rows, preferred_element_type=jnp.float32)  4.49 us
    dot_general x1, matrix products, shards(): jnp.dot(normed, pool_weight.reshape(width, -1), preferred_element_type=jn...  3.68 us
  transfers between devices with their start and end apart: 5, of which 2 were waited for; matrix products, arithmetic and copies ran while one was open for 31% of the time, Pallas kernels for 0%

profile of v1, /device:TPU:0, one launch (start us, length us, event | category | flops | bytes accessed | tf_op | source)
XLA Modules:
  0.0 110.1 jit_solution(18215774276980217313)
XLA Ops:
  11.1 1.5 %broadcast_compare_fusion = pred[768,896]{1,0:T(8,128)(4,1)} fusion(s32[768]{0:T(1024)S(1)} %iota_add_fusion), kind=kLoop, calls=%fused_computation.33 | loop fusion | flops 2064384 | bytes 691200 | tf_op jit(solution)/shard_map/ge | solution.py:109
  12.6 1.8 %subtract_convert_fusion = f32[768,896]{1,0:T(8,128)} fusion(s32[768]{0:T(1024)S(1)} %iota_add_fusion), kind=kLoop, calls=%fused_computation.21 | loop fusion | flops 1376256 | bytes 2755584 | tf_op jit(solution)/shard_map/convert_element_type | solution.py:106
  14.3 9.4 %all-gather.5.cloned.1.call-done = bf16[2,768,1024]{2,1,0:T(8,128)(2,1)} async-done(((bf16[1,768,1024]{2,1,0:T(8,128)(2,1)}), bf16[2,768,1024]{2,1,0:T(8,128)(2,1)}) %all-gather.5.cloned.1.call-update) | async-done | bytes 3145744 | tf_op jit(solution)/shard_map/all_gather | solution.py:69
  23.8 4.6 %copy.26 = bf16[2,768,1024]{1,2,0:T(8,128)(2,1)} copy(bf16[2,768,1024]{2,1,0:T(8,128)(2,1)} %all-gather.5.cloned.1.call-done) | data formatting | bytes 6291456 | tf_op jit(solution)/shard_map/all_gather | solution.py:69
  28.4 2.7 %fusion.4 = f32[768]{0:T(1024)S(1)} fusion(bf16[2,768,1024]{1,2,0:T(8,128)(2,1)} %copy.26), kind=kLoop, calls=%fused_computation.6 | loop fusion | flops 4717824 | bytes 3148800 | tf_op jit(solution)/shard_map/reduce_sum | solution.py:17
  31.2 0.8 fusion.6
  32.0 1.6 %copy-done.2 = bf16[2,1,768,1024]{2,3,0,1:T(8,128)(2,1)} copy-done((bf16[2,1,768,1024]{2,3,0,1:T(8,128)(2,1)}, bf16[2,1,768,1024]{2,3,0,1:T(8,128)(2,1)S(1)}, u32[]{:S(2)}) %copy-start.2) | copy-done | bytes 3145752
  34.5 4.5 %collective-permute-start = (bf16[128,2,64]{0,2,1:T(8,128)(2,1)S(1)}, bf16[128,2,64]{0,2,1:T(8,128)(2,1)}, u32[]{:S(2)}, u32[]{:S(2)}) collective-permute-start(bf16[128,2,64]{0,2,1:T(8,128)(2,1)S(1)} %bitcast.109), channel_id=1, source_target_pairs={{0,4},{4,8},{8,12},{1,5},{5,9},{9,13},{2,6},{6,10},{10,14},{3,7},{... | collective-permute-start | bytes 98312 | tf_op jit(solution)/shard_map/ppermute | solution.py:12
  39.0 2.5 %convolution_convert_fusion.1 = bf16[768,128]{0,1:T(8,128)(2,1)S(1)} fusion(bf16[2048,128]{0,1:T(8,128)(2,1)S(1)} %bitcast.105, bf16[768,2048]{0,1:T(8,128)(2,1)} %bitcast.98), kind=kOutput, calls=%fused_computation.35 | convolution fusion | flops 402751488 | bytes 3866624 | tf_op jit(solution)/shard_map/dot_general | solution.py:79
  41.5 3.4 %collective-permute-start.1 = (bf16[128,2,64]{0,2,1:T(8,128)(2,1)S(1)}, bf16[128,2,64]{0,2,1:T(8,128)(2,1)}, u32[]{:S(2)}, u32[]{:S(2)}) collective-permute-start(bf16[128,2,64]{0,2,1:T(8,128)(2,1)S(1)} %bitcast.110), channel_id=1, source_target_pairs={{0,4},{4,8},{8,12},{1,5},{5,9},{9,13},{2,6},{6,10},{10,14},{3,7},{... | collective-permute-start | bytes 98312 | tf_op jit(solution)/shard_map/ppermute | solution.py:12
  45.0 3.7 %fusion.24 = bf16[768,512]{0,1:T(8,128)(2,1)S(1)} fusion(bf16[768,2048]{0,1:T(8,128)(2,1)S(1)} %bitcast.99, bf16[256,8,4,128]{3,2,1,0:T(4,128)(2,1)} %bitcast.114), kind=kOutput, calls=%fused_computation.30 | convolution fusion | flops 1611005952 | bytes 6029312 | tf_op jit(solution)/shard_map/dot_general | solution.py:85
  48.7 2.7 %convolution_convert_fusion = bf16[768,512]{1,0:T(8,128)(2,1)} fusion(bf16[768,2048]{0,1:T(8,128)(2,1)S(1)} %bitcast.100, bf16[2048,512]{0,1:T(8,128)(2,1)S(1)} %bitcast.115), kind=kOutput, calls=%fused_computation.31 | convolution fusion | flops 1611005952 | bytes 6029312 | tf_op jit(solution)/shard_map/dot_general | solution.py:76
  51.6 8.5 %all-gather.2 = f32[4,1,128]{2,1,0:T(1,128)S(1)} all-gather(f32[1,1,128]{2,1,0:T(1,128)S(1)} %bitcast.112), channel_id=3, replica_groups=mesh['grp'=2,'sp'=4,'fs'=2,'tp'=2] {'sp'}, dimensions={0}, use_global_device_ids=true | all-gather | bytes 2560 | tf_op jit(solution)/shard_map/all_gather | solution.py:99
  60.1 3.7 %collective-permute-start.2 = (bf16[128,4,128]{0,2,1:T(8,128)(2,1)S(1)}, bf16[128,4,128]{0,2,1:T(8,128)(2,1)}, u32[]{:S(2)}, u32[]{:S(2)}) collective-permute-start(bf16[128,4,128]{0,2,1:T(8,128)(2,1)S(1)} %bitcast.108), channel_id=1, source_target_pairs={{0,4},{4,8},{8,12},{1,5},{5,9},{9,13},{2,6},{6,10},{10,14},{3,7},{... | collective-permute-start | bytes 393224 | tf_op jit(solution)/shard_map/ppermute | solution.py:12
  64.7 3.6 %reshape.335 = bf16[6,128,2,4,64]{4,3,2,1,0:T(4,128)(2,1)} reshape(bf16[768,512]{1,0:T(8,128)(2,1)} %convolution_convert_fusion) | data formatting | bytes 1572864 | tf_op jit(solution)/shard_map/reshape | solution.py:27
  68.3 1.2 %concatenate.23 = f32[4,128]{1,0:T(4,128)} pad(f32[1,128]{1,0:T(1,128)} %bitcast.113, f32[]{:T(128)} %constant.14.clone.1), padding=3_0x0_0 | pad | bytes 2564 | tf_op jit(solution)/shard_map/concatenate | solution.py:116
  69.5 0.8 copy_bitcast_fusion
  70.3 2.7 %fusion.13 = (f32[6,2,4,128]{3,2,1,0:T(4,128)S(1)}, f32[6,2,256,128,4]{3,2,4,1,0:T(8,128)S(1)}) fusion(pred[6,128,256]{1,2,0:T(8,128)(4,1)S(1)} %broadcast_and_fusion, bf16[6,128,2,4,64]{4,3,2,1,0:T(4,128)(2,1)} %reshape.335, bf16[6,128,2,64]{1,3,2,0:T(8,128)(2,1)S(1)} %copy.30, bf16[6,128,2,64]{1,3,2,0:T(8,128)(2,1)S(1)} %copy_bitcast_fusion), kind=kOutput, calls=%fused_computation.19 | convolution fusion | flops 206825472 | bytes 7692288 | tf_op jit(solution)/shard_map/nqhgd,nkhd->nhgqk/dot_general | solution.py:45
  73.1 1.7 %fusion.8 = f32[6,2,4,128]{3,2,1,0:T(4,128)S(1)} fusion(f32[6,2,256,128,4]{3,2,4,1,0:T(8,128)S(1)} %get-tuple-element.6, f32[6,2,4,128]{3,2,1,0:T(4,128)S(1)} %broadcast_maximum_fusion, pred[6,128,256]{1,2,0:T(8,128)(4,1)S(1)} %broadcast_and_fusion), kind=kLoop, calls=%fused_computation.14 | loop fusion | flops 6285312 | bytes 6537216 | tf_op jit(solution)/shard_map/reduce_sum | solution.py:52
  74.8 0.8 copy_bitcast_fusion.1
  75.6 1.7 %fusion.30 = bf16[6,128,2,4,64]{1,4,3,2,0:T(8,128)(2,1)S(1)} fusion(f32[6,2,256,128,4]{3,2,4,1,0:T(8,128)S(1)} %get-tuple-element.6, f32[6,2,4,128]{3,2,1,0:T(4,128)S(1)} %exponential_add_fusion, f32[6,2,4,128]{3,2,1,0:T(4,128)S(1)} %broadcast_maximum_fusion, pred[6,128,256]{1,2,0:T(8,128)(4,1)S(1)} %broadcast_and_fusion, ...), kind=kOutput, calls=%fused_computation.34 | convolution fusion | flops 210370560 | bytes 7716864 | tf_op jit(solution)/shard_map/nhgqk,nkhd->nqhgd/dot_general | solution.py:54
  78.0 4.5 %fusion.37 = f32[768,2048]{1,0:T(8,128)} fusion(bf16[512,2048]{1,0:T(8,128)(2,1)S(1)} %bitcast.96, bf16[64,8,6,128]{3,2,1,0:T(8,128)(2,1)S(1)} %bitcast.101), kind=kOutput, calls=%fused_computation.40 | convolution fusion | flops 1610612736 | bytes 9175040 | tf_op jit(solution)/shard_map/dot_general | solution.py:127
  82.5 11.3 %fusion.7 = bf16[768,2048]{1,0:T(8,128)(2,1)} fusion(f32[768,2048]{1,0:T(8,128)} %fusion.37, bf16[4,128,2048]{2,1,0:T(8,128)(2,1)} %param.18, bf16[768,4,128]{0,2,1:T(8,128)(2,1)} %bitcast.107, f32[768,896]{1,0:T(8,128)} %subtract_convert_fusion, f32[4]{0:T(128)S(1)} %copy-done.10, pred[4,896]{1,0:T(4,128)(4,1)S(1)} %copy-done.8, ...), kind=kOutput, calls=%fused_computation.10 | convolution fusion | flops 2330460160 | bytes 15910416 | tf_op jit(solution)/shard_map/dot_general | solution.py:129
  93.8 9.5 %reduce-scatter.2.cloned.1.call-done = bf16[384,2048]{1,0:T(8,128)(2,1)} async-done(((bf16[768,2048]{1,0:T(8,128)(2,1)}), bf16[384,2048]{1,0:T(8,128)(2,1)}) %reduce-scatter.2.cloned.1.call-update) | async-done | bytes 1572880 | tf_op jit(solution)/shard_map/reduce_scatter | solution.py:128
  (60 shorter events, 7.3 us)
Async XLA Ops:
  6.5 71.4 %copy-start = (bf16[8,64,2048]{2,1,0:T(8,128)(2,1)S(1)}, bf16[8,64,2048]{2,1,0:T(8,128)(2,1)}, u32[]{:S(2)}) copy-start(bf16[8,64,2048]{2,1,0:T(8,128)(2,1)} %param.17) | copy-start | bytes 6291460
  6.5 17.2 %all-gather.5.cloned.1.call-start = ((), (), s32[]{:S(2)}) async-start(), calls=%async_computation.2 | async-start | bytes 4718592 | tf_op jit(solution)/shard_map/all_gather | solution.py:69
  7.3 96.0 %reduce-scatter.2.cloned.1.call-start = ((), (), s32[]{:S(2)}) async-start(), calls=%async_computation.1 | async-start | bytes 4718592 | tf_op jit(solution)/shard_map/reduce_scatter | solution.py:128
  28.4 2.8 %copy-start.1 = (bf16[2,768,1024]{1,2,0:T(8,128)(2,1)S(1)}, bf16[2,768,1024]{1,2,0:T(8,128)(2,1)}, u32[]{:S(2)}) copy-start(bf16[2,768,1024]{1,2,0:T(8,128)(2,1)} %copy.26) | copy-start | bytes 9437188
  31.2 2.4 %copy-start.5 = (bf16[2048,2,64]{0,2,1:T(8,128)(2,1)S(1)}, bf16[2048,2,64]{0,2,1:T(8,128)(2,1)}, u32[]{:S(2)}) copy-start(bf16[2048,2,64]{0,2,1:T(8,128)(2,1)} %param.14) | copy-start | bytes 1572868
  32.0 1.7 %copy-start.2 = (bf16[2,1,768,1024]{2,3,0,1:T(8,128)(2,1)}, bf16[2,1,768,1024]{2,3,0,1:T(8,128)(2,1)S(1)}, u32[]{:S(2)}) copy-start(bf16[2,1,768,1024]{2,3,0,1:T(8,128)(2,1)S(1)} %fusion.6) | copy-start | bytes 9437188
  32.0 7.0 %copy-start.6 = (bf16[2048,2,64]{0,2,1:T(8,128)(2,1)S(1)}, bf16[2048,2,64]{0,2,1:T(8,128)(2,1)}, u32[]{:S(2)}) copy-start(bf16[2048,2,64]{0,2,1:T(8,128)(2,1)} %param.13) | copy-start | bytes 1572868
  34.5 10.5 %copy-start.3 = (bf16[2,1,768,1024]{2,3,0,1:T(8,128)(2,1)S(1)}, bf16[2,1,768,1024]{2,3,0,1:T(8,128)(2,1)}, u32[]{:S(2)}) copy-start(bf16[2,1,768,1024]{2,3,0,1:T(8,128)(2,1)} %copy-done.2) | copy-start | bytes 9437188
  34.5 40.3 %collective-permute-start = (bf16[128,2,64]{0,2,1:T(8,128)(2,1)S(1)}, bf16[128,2,64]{0,2,1:T(8,128)(2,1)}, u32[]{:S(2)}, u32[]{:S(2)}) collective-permute-start(bf16[128,2,64]{0,2,1:T(8,128)(2,1)S(1)} %bitcast.109), channel_id=1, source_target_pairs={{0,4},{4,8},{8,12},{1,5},{5,9},{9,13},{2,6},{6,10},{10,14},{3,7},{... | collective-permute-start | bytes 98312 | tf_op jit(solution)/shard_map/ppermute | solution.py:12
  41.5 28.0 %collective-permute-start.1 = (bf16[128,2,64]{0,2,1:T(8,128)(2,1)S(1)}, bf16[128,2,64]{0,2,1:T(8,128)(2,1)}, u32[]{:S(2)}, u32[]{:S(2)}) collective-permute-start(bf16[128,2,64]{0,2,1:T(8,128)(2,1)S(1)} %bitcast.110), channel_id=1, source_target_pairs={{0,4},{4,8},{8,12},{1,5},{5,9},{9,13},{2,6},{6,10},{10,14},{3,7},{... | collective-permute-start | bytes 98312 | tf_op jit(solution)/shard_map/ppermute | solution.py:12
  45.0 3.7 %copy-start.12 = (bf16[2048,8,64]{0,2,1:T(8,128)(2,1)S(1)}, bf16[2048,8,64]{0,2,1:T(8,128)(2,1)}, u32[]{:S(2)}) copy-start(bf16[2048,8,64]{0,2,1:T(8,128)(2,1)} %param.12) | copy-start | bytes 6291460
  48.7 2.8 %copy-start.7 = (bf16[768,512]{0,1:T(8,128)(2,1)}, bf16[768,512]{0,1:T(8,128)(2,1)S(1)}, u32[]{:S(2)}) copy-start(bf16[768,512]{0,1:T(8,128)(2,1)S(1)} %fusion.24) | copy-start | bytes 2359300
  48.7 15.0 %copy-start.11 = (pred[4]{0:T(512)(128)(4,1)S(1)}, pred[4]{0:T(512)(128)(4,1)}, u32[]{:S(2)}) copy-start(pred[4]{0:T(512)(128)(4,1)} %iota_compare_fusion.1) | copy-start | bytes 16
  60.1 22.4 %collective-permute-start.2 = (bf16[128,4,128]{0,2,1:T(8,128)(2,1)S(1)}, bf16[128,4,128]{0,2,1:T(8,128)(2,1)}, u32[]{:S(2)}, u32[]{:S(2)}) collective-permute-start(bf16[128,4,128]{0,2,1:T(8,128)(2,1)S(1)} %bitcast.108), channel_id=1, source_target_pairs={{0,4},{4,8},{8,12},{1,5},{5,9},{9,13},{2,6},{6,10},{10,14},{3,7},{... | collective-permute-start | bytes 393224 | tf_op jit(solution)/shard_map/ppermute | solution.py:12
  77.9 4.5 %copy-start.4 = (pred[768,896]{1,0:T(8,128)(4,1)S(1)}, pred[768,896]{1,0:T(8,128)(4,1)}, u32[]{:S(2)}) copy-start(pred[768,896]{1,0:T(8,128)(4,1)} %broadcast_compare_fusion) | copy-start | bytes 2064388
  78.0 4.5 %copy-start.8 = (pred[4,896]{1,0:T(4,128)(4,1)S(1)}, pred[4,896]{1,0:T(4,128)(4,1)}, u32[]{:S(2)}) copy-start(pred[4,896]{1,0:T(4,128)(4,1)} %broadcast_or_fusion) | copy-start | bytes 10756
  78.0 4.5 %copy-start.9 = (f32[4,128]{1,0:T(4,128)S(1)}, f32[4,128]{1,0:T(4,128)}, u32[]{:S(2)}) copy-start(f32[4,128]{1,0:T(4,128)} %concatenate.23) | copy-start | bytes 6148
  78.0 4.5 %copy-start.10 = (f32[4]{0:T(128)S(1)}, f32[4]{0:T(128)}, u32[]{:S(2)}) copy-start(f32[4]{0:T(128)} %constant.13.clone) | copy-start | bytes 52
Sparse Core Ops, SparseCore 0:
  8.9 14.8 all-gather.4
  94.0 9.2 reduce-scatter.1
